TPU v7x, 32 devices: a whole 2x2x4 slice. The times are simulated.
32 devices in a mesh: sp: 8 (over z, y), tp: 4 (over x, core).
Axes of the slice: x: 2, y: 2, z: 4, core: 2. Of those that a mesh axis runs over, the one named last changes fastest.
Arguments:
- layer_input: bfloat16 [8, 1024, 2048], P(None, ('sp', 'tp')), may hold values from -6 to 6
- input_gain: float32 [2048], replicated, may hold values from 0.5 to 1.5
- narrowing_matrix: bfloat16 [2048, 512], replicated, may hold values from -0.125 to 0.125
- rotary_down: bfloat16 [2048, 64], replicated, may hold values from -0.125 to 0.125
- summary_scaling: float32 [512], replicated, may hold values from 0.5 to 1.5
- lookup_widening: bfloat16 [512, 16, 128], P('tp'), may hold values from -0.25 to 0.25
- payload_widening: bfloat16 [512, 16, 128], P('tp'), may hold values from -0.25 to 0.25
- query_nope: bfloat16 [8, 16, 128], P('sp', 'tp'), may hold values from -6 to 6
- query_rotary: bfloat16 [8, 16, 64], P('sp', 'tp'), may hold values from -6 to 6
Outputs:
- stored_summaries: bfloat16 [8, 1024, 512], P('sp', None, 'tp')
- rotary_cache: bfloat16 [8, 1024, 64], P('sp', None, 'tp')
- first_read: bfloat16 [8, 16, 128], P('sp', 'tp')
All inputs are finite; a program needn't handle non-finite values.
Results may differ from a plain program's by a relative error of at most 0.02.
Values may be sent and summed in bfloat16 or wider, within the bound.
A program may use at most 64 MiB of HBM per device.

v0:
```python
import jax
import jax.numpy as jnp
from jax import lax
from jax.sharding import PartitionSpec as P

QK_ROPE = 64
PLAIN_MATCH_SPAN = 128
norm_eps = 1e-06
rotary_base = 10000.0


def summed_rows(portion, width, axis):
    count = width * lax.axis_size(axis)
    return lax.psum_scatter(portion(jnp.int32(0), count), axis, scatter_dimension=0, tiled=True)


def rescaled_lines(vector):
    return vector * lax.rsqrt(jnp.mean(vector * vector, axis=-1, keepdims=True) + norm_eps)


def rotate(vector, position):
    half_width = vector.shape[-1] // 2
    frequency = 1.0 / rotary_base ** (
        jnp.arange(half_width, dtype=jnp.float32) * 2.0 / vector.shape[-1]
    )
    angles = position * frequency
    first_half = vector[..., :half_width]
    second_half = vector[..., half_width:]
    return jnp.concatenate(
        [
            first_half * jnp.cos(angles) - second_half * jnp.sin(angles),
            second_half * jnp.cos(angles) + first_half * jnp.sin(angles),
        ],
        axis=-1,
    )


def to_pieces(array, sp_count, tp_count):
    seq_count, pos_local, cache_width = array.shape
    seq_each = seq_count // sp_count
    width_each = cache_width // tp_count
    array = array.reshape(sp_count, seq_each, pos_local, tp_count, width_each)
    array = array.transpose(0, 3, 1, 2, 4)
    return array.reshape(sp_count * tp_count, seq_each, pos_local, width_each)


def shards(
    layer_input,
    input_gain,
    narrowing_matrix,
    rotary_down,
    summary_scaling,
    lookup_widening,
    payload_widening,
    query_nope,
    query_rotary,
):
    seq_count, pos_local, feature_width = layer_input.shape
    sp_count = lax.axis_size("sp")
    tp_count = lax.axis_size("tp")
    block_index = lax.axis_index(("sp", "tp"))
    normed = (rescaled_lines(layer_input.astype(jnp.float32)) * input_gain).astype(jnp.bfloat16)
    flat_rows = normed.reshape(seq_count * pos_local, feature_width)
    hidden_summary = jnp.dot(
        flat_rows, narrowing_matrix, preferred_element_type=jnp.float32
    ).astype(jnp.bfloat16)
    rotary = jnp.dot(flat_rows, rotary_down, preferred_element_type=jnp.float32).astype(
        jnp.bfloat16
    )
    hidden_summary = (
        (rescaled_lines(hidden_summary.astype(jnp.float32)) * summary_scaling)
        .astype(jnp.bfloat16)
        .reshape(seq_count, pos_local, -1)
    )
    positions = (block_index * pos_local + jnp.arange(pos_local, dtype=jnp.int32)).astype(
        jnp.float32
    )[None, :, None]
    rotary = rotate(rotary.astype(jnp.float32).reshape(seq_count, pos_local, -1), positions).astype(
        jnp.bfloat16
    )
    moved = (
        lax.all_to_all(
            to_pieces(hidden_summary, sp_count, tp_count),
            ("sp", "tp"),
            split_axis=0,
            concat_axis=2,
            tiled=True,
        ),
        lax.all_to_all(
            to_pieces(rotary, sp_count, tp_count),
            ("sp", "tp"),
            split_axis=0,
            concat_axis=2,
            tiled=True,
        ),
    )
    hidden_summary = moved[0][0]
    rotary = moved[1][0]
    pos_total = hidden_summary.shape[1]
    rot_each = rotary.shape[2]
    head_each = query_nope.shape[1]
    query_all, turn_all = (
        lax.all_gather(query_nope, "tp", axis=1, tiled=True),
        lax.all_gather(query_rotary, "tp", axis=1, tiled=True),
    )
    absorbed = jnp.einsum(
        "shd,chd->shc", query_all, lookup_widening, preferred_element_type=jnp.float32
    ).astype(jnp.bfloat16)
    query_turned = rotate(turn_all.astype(jnp.float32), jnp.float32(pos_total)).astype(jnp.bfloat16)
    turned_mine = lax.dynamic_slice_in_dim(
        query_turned, lax.axis_index("tp") * rot_each, rot_each, 2
    )
    score_scale = (PLAIN_MATCH_SPAN + QK_ROPE) ** (-0.5)
    partial_value = (
        jnp.einsum("shc,spc->shp", absorbed, hidden_summary, preferred_element_type=jnp.float32)
        + jnp.einsum("shr,spr->shp", turned_mine, rotary, preferred_element_type=jnp.float32)
    ) * score_scale
    scores = lax.psum(partial_value.astype(jnp.bfloat16), "tp").astype(jnp.float32)
    attention = jax.nn.softmax(scores, axis=-1).astype(jnp.bfloat16)
    context = jnp.einsum(
        "shp,spc->shc", attention, hidden_summary, preferred_element_type=jnp.float32
    ).astype(jnp.bfloat16)

    def project_heads(row_start, row_count):
        part_context = lax.dynamic_slice_in_dim(context, row_start, row_count, 1)
        part_weight = lax.dynamic_slice_in_dim(payload_widening, row_start, row_count, 1)
        return jnp.einsum(
            "shc,chv->hsv", part_context, part_weight, preferred_element_type=jnp.float32
        )

    values = summed_rows(project_heads, head_each, "tp")
    first_read = rescaled_lines(values.transpose(1, 0, 2)).astype(jnp.bfloat16)
    return (hidden_summary, rotary, first_read)


def solution(mesh):
    return jax.shard_map(
        shards,
        mesh=mesh,
        in_specs=(
            P(None, ("sp", "tp"), None),
            P(),
            P(),
            P(),
            P(),
            P("tp", None, None),
            P("tp", None, None),
            P("sp", "tp", None),
            P("sp", "tp", None),
        ),
        out_specs=(P("sp", None, "tp"), P("sp", None, "tp"), P("sp", "tp", None)),
        check_vma=False,
    )
```

profile of v0, /device:TPU:0, one launch (start us, length us, event | category | flops | bytes accessed | tf_op | source)
XLA Modules:
  0.0 55.6 jit_solution(11520406021461989264)
XLA Ops:
  0.7 1.7 %fusion = f32[8,32]{1,0:T(8,128)S(1)} fusion(bf16[8,32,2048]{2,1,0:T(8,128)(2,1)} %param.9), kind=kLoop, calls=%fused_computation.2 | loop fusion | flops 1572608 | bytes 1049600 | tf_op jit(solution)/shard_map/reduce_sum | solution.py:18
  2.4 1.5 %fusion.2 = bf16[8,32,2048]{2,1,0:T(8,128)(2,1)S(1)} fusion(bf16[8,32,2048]{2,1,0:T(8,128)(2,1)} %param.9, f32[2048]{0:T(1024)} %param.10, f32[8,32]{1,0:T(8,128)S(1)} %add_rsqrt_fusion), kind=kLoop, calls=%fused_computation.4 | loop fusion | flops 2097152 | bytes 2106368 | tf_op jit(solution)/shard_map/convert_element_type | solution.py:62
  4.0 0.4 fusion.6
  4.5 0.1 multiply_cosine_fusion
  4.6 0.1 subtract_convert_fusion
  4.9 0.1 copy.34
  5.0 0.8 %reshape.300 = bf16[32,2,256]{2,1,0:T(2,128)(2,1)} reshape(bf16[32,1,16,32]{3,2,1,0:T(8,128)(2,1)S(1)} %bitcast.62) | data formatting | bytes 65536
  5.8 7.3 %all-to-all-start.1 = ((bf16[32,2,256]{2,1,0:T(2,128)(2,1)}), bf16[32,2,256]{2,1,0:T(2,128)(2,1)S(1)}, u32[]{:S(2)}, u32[]{:S(2)}) async-start(bf16[32,2,256]{2,1,0:T(2,128)(2,1)} %reshape.300), calls=%async_computation.1 | async-start | bytes 65536 | tf_op jit(solution)/shard_map/all_to_all | solution.py:89
  13.1 5.2 %all_gather.7 = bf16[1,16,64]{2,0,1:T(2,128)(2,1)S(1)} all-gather(bf16[1,4,64]{2,0,1:T(2,128)(2,1)S(1)} %copy.37), channel_id=1, replica_groups=mesh['sp'=8,'tp'=4] {'tp'}, dimensions={1}, use_global_device_ids=true | all-gather | bytes 2560 | tf_op jit(solution)/shard_map/all_gather | solution.py:104
  18.3 0.8 %multiply_reduce_fusion = (f32[256]{0:T(256)S(1)}, f32[256,512]{1,0:T(8,128)S(1)}) fusion(bf16[256,2048]{1,0:T(8,128)(2,1)S(1)} %bitcast.57, bf16[2048,512]{1,0:T(8,128)(2,1)S(1)} %copy-done), kind=kOutput, calls=%fused_computation.20 | convolution fusion | flops 537394944 | bytes 3671040 | tf_op jit(solution)/shard_map/dot_general | solution.py:64
  19.2 0.1 multiply_convert_fusion
  19.4 0.8 %copy.31 = bf16[8,1,32,4,128]{4,2,3,0,1:T(8,128)(2,1)} copy(bf16[8,1,32,4,128]{4,3,2,0,1:T(4,128)(2,1)S(1)} %reshape_reshape.3) | data formatting | bytes 524288 | tf_op jit(solution)/shard_map/reshape;reshape | solution.py:42
  20.1 0.2 all-to-all-done.1
  20.4 5.6 %all-to-all-start = ((bf16[32,1,32,128]{3,2,1,0:T(8,128)(2,1)}), bf16[32,1,32,128]{3,2,1,0:T(8,128)(2,1)S(1)}, u32[]{:S(2)}, u32[]{:S(2)}) async-start(bf16[32,1,32,128]{3,2,1,0:T(8,128)(2,1)} %bitcast.3), calls=%async_computation | async-start | bytes 524288 | tf_op jit(solution)/shard_map/all_to_all | solution.py:82
  26.1 0.6 %dynamic-slice = u32[1]{0:T(128)} dynamic-slice(u32[32]{0:T(128)S(1)} %copy-done.7, u32[]{:T(128)S(6)} %add.73), dynamic_slice_sizes={1} | dynamic-slice | bytes 12
  27.3 5.2 %all_gather.6 = bf16[1,16,128]{2,0,1:T(2,128)(2,1)S(1)} all-gather(bf16[1,4,128]{2,0,1:T(2,128)(2,1)S(1)} %copy.36), channel_id=1, replica_groups=mesh['sp'=8,'tp'=4] {'tp'}, dimensions={1}, use_global_device_ids=true | all-gather | bytes 5120 | tf_op jit(solution)/shard_map/all_gather | solution.py:103
  32.6 0.4 fusion.11
  33.0 0.2 reshape.301
  33.2 0.2 reshape.287
  33.3 0.8 %squeeze.7 = bf16[1,1024,16]{1,2,0:T(8,128)(2,1)} reshape(bf16[32,1,32,16]{2,0,3,1:T(8,128)(2,1)S(1)} %copy.35) | data formatting | bytes 65536 | tf_op jit(solution)/shard_map/squeeze | solution.py:98
  34.1 2.4 %all-to-all-done = bf16[32,1,32,128]{3,2,1,0:T(8,128)(2,1)S(1)} async-done(((bf16[32,1,32,128]{3,2,1,0:T(8,128)(2,1)}), bf16[32,1,32,128]{3,2,1,0:T(8,128)(2,1)S(1)}, u32[]{:S(2)}, u32[]{:S(2)}) %all-to-all-start) | async-done | bytes 262176 | tf_op jit(solution)/shard_map/all_to_all | solution.py:82
  36.5 0.2 fusion.25
  36.7 0.2 fusion.7
  36.9 10.6 %psum.7 = bf16[1,16,1024]{2,1,0:T(8,128)(2,1)S(1)} all-reduce(bf16[1,16,1024]{2,1,0:T(8,128)(2,1)S(1)} %fusion.7), channel_id=1, replica_groups=mesh['sp'=8,'tp'=4] {'tp'}, use_global_device_ids=true, to_apply=%region_2.0 | all-reduce | flops 16384 | bytes 65536 | tf_op jit(solution)/shard_map/psum | solution.py:118
  47.5 0.1 reduce_max.14
  47.7 0.2 fusion.13
  47.9 0.2 fusion.8
  48.1 0.3 fusion.9
  48.3 5.8 %all-reduce = f32[16,1,128]{2,0,1:T(8,128)S(1)} all-reduce(f32[16,1,128]{2,0,1:T(8,128)S(1)} %bitcast.64), channel_id=2, replica_groups=mesh['sp'=8,'tp'=4] {'tp'}, use_global_device_ids=true, to_apply=%region_5.0.clone | all-reduce | flops 2048 | bytes 16384
  54.1 0.1 multiply_reduce_fusion.1
  54.2 0.6 %multiply_convert_fusion.1 = bf16[1,4,128]{2,1,0:T(4,128)(2,1)} fusion(f32[16,1,128]{2,0,1:T(8,128)S(1)} %all-reduce, u32[]{:T(128)S(6)} %multiply.33, f32[4]{0:T(128)S(1)} %add_rsqrt_fusion.2), kind=kLoop, calls=%fused_computation.46 | loop fusion | flops 1024 | bytes 3092 | tf_op jit(solution)/shard_map/convert_element_type | solution.py:132
  54.9 0.7 %copy.56 = bf16[1,1024,128]{2,1,0:T(8,128)(2,1)} copy(bf16[1,1024,128]{2,1,0:T(8,128)(2,1)S(1)} %bitcast.60) | data formatting | bytes 524288
  (31 shorter events, 0.5 us)
Async XLA Ops:
  0.6 17.7 %copy-start = (bf16[2048,512]{1,0:T(8,128)(2,1)S(1)}, bf16[2048,512]{1,0:T(8,128)(2,1)}, u32[]{:S(2)}) copy-start(bf16[2048,512]{1,0:T(8,128)(2,1)} %param.11) | copy-start | bytes 6291460
  0.6 3.3 %copy-start.1 = (bf16[2048,64]{0,1:T(8,128)(2,1)S(1)}, bf16[2048,64]{0,1:T(8,128)(2,1)}, u32[]{:S(2)}) copy-start(bf16[2048,64]{0,1:T(8,128)(2,1)} %param.12) | copy-start | bytes 786436
  2.4 10.7 %copy-start.3 = (bf16[1,4,64]{2,1,0:T(4,128)(2,1)S(1)}, bf16[1,4,64]{2,1,0:T(4,128)(2,1)}, u32[]{:S(2)}) copy-start(bf16[1,4,64]{2,1,0:T(4,128)(2,1)} %param.17) | copy-start | bytes 1540
  5.0 14.2 %copy-start.2 = (f32[512]{0:T(512)S(1)}, f32[512]{0:T(512)}, u32[]{:S(2)}) copy-start(f32[512]{0:T(512)} %param.13) | copy-start | bytes 6148
  5.8 14.6 %all-to-all-start.1 = ((bf16[32,2,256]{2,1,0:T(2,128)(2,1)}), bf16[32,2,256]{2,1,0:T(2,128)(2,1)S(1)}, u32[]{:S(2)}, u32[]{:S(2)}) async-start(bf16[32,2,256]{2,1,0:T(2,128)(2,1)} %reshape.300), calls=%async_computation.1 | async-start | bytes 65536 | tf_op jit(solution)/shard_map/all_to_all | solution.py:89
  19.1 6.9 %copy-start.4 = (bf16[1,4,128]{2,1,0:T(4,128)(2,1)S(1)}, bf16[1,4,128]{2,1,0:T(4,128)(2,1)}, u32[]{:S(2)}) copy-start(bf16[1,4,128]{2,1,0:T(4,128)(2,1)} %param.16) | copy-start | bytes 3076
  19.1 7.0 %copy-start.7 = (u32[32]{0:T(128)S(1)}, u32[32]{0:T(128)}, u32[]{:S(2)}) copy-start(u32[32]{0:T(128)} %constant.54) | copy-start | bytes 388
  19.1 13.5 %copy-start.5 = (bf16[128,16,128]{2,1,0:T(8,128)(2,1)S(1)}, bf16[128,16,128]{2,1,0:T(8,128)(2,1)}, u32[]{:S(2)}) copy-start(bf16[128,16,128]{2,1,0:T(8,128)(2,1)} %param.14) | copy-start | bytes 1572868
  19.4 28.7 %copy-start.6 = (bf16[128,16,128]{2,1,0:T(8,128)(2,1)S(1)}, bf16[128,16,128]{2,1,0:T(8,128)(2,1)}, u32[]{:S(2)}) copy-start(bf16[128,16,128]{2,1,0:T(8,128)(2,1)} %param.15) | copy-start | bytes 1572868
  20.4 16.2 %all-to-all-start = ((bf16[32,1,32,128]{3,2,1,0:T(8,128)(2,1)}), bf16[32,1,32,128]{3,2,1,0:T(8,128)(2,1)S(1)}, u32[]{:S(2)}, u32[]{:S(2)}) async-start(bf16[32,1,32,128]{3,2,1,0:T(8,128)(2,1)} %bitcast.3), calls=%async_computation | async-start | bytes 524288 | tf_op jit(solution)/shard_map/all_to_all | solution.py:82
where the time goes:
time: 55.9 us; the launch traced here: 55.6 us
  blocking collectives  26.7 us (48%)
  starting transfers between devices  12.9 us (23%)
  other arithmetic  4.95 us (9%)
  local copies, waits for them, and re-layouts  4.3 us (8%)
  waiting for transfers between devices  2.64 us (5%)
  matrix products  2.46 us (4%)
  between operations  1.56 us (3%)
    psum x1, blocking collectives, shards(): lax.psum(partial_value.astype(jnp.bfloat16), 'tp').astype(jnp.float32)  10.6 us
    all_to_all x1, starting transfers between devices, shards(): lax.all_to_all(to_pieces(rotary, sp_count, tp_count), ('sp', 'tp'), split...  7.33 us
    unnamed x1, blocking collectives  5.76 us
    all_to_all x1, starting transfers between devices, shards(): lax.all_to_all(to_pieces(hidden_summary, sp_count, tp_count), ('sp', 'tp'...  5.61 us
    all_gather x1, blocking collectives, shards(): lax.all_gather(query_nope, 'tp', axis=1, tiled=True)  5.2 us
    all_gather x1, blocking collectives, shards(): lax.all_gather(query_rotary, 'tp', axis=1, tiled=True)  5.19 us
    all_to_all x1, waiting for transfers between devices, shards(): lax.all_to_all(to_pieces(hidden_summary, sp_count, tp_count), ('sp', 'tp'...  2.41 us
    unnamed x22, local copies, waits for them, and re-layouts  2.26 us
  transfers between devices with their start and end apart: 2, of which 2 were waited for; matrix products, arithmetic and copies ran while one was open for 7% of the time, Pallas kernels for 0%

commit v1 on v0

--- a/solution.py
+++ b/solution.py
@@ -79,12 +79,20 @@
         jnp.bfloat16
     )
     moved = (
-        lax.all_to_all(
-            to_pieces(hidden_summary, sp_count, tp_count),
-            ("sp", "tp"),
-            split_axis=0,
-            concat_axis=2,
-            tiled=True,
+        jnp.concatenate(
+            lax.all_to_all(
+                jnp.stack(
+                    jnp.split(
+                        to_pieces(hidden_summary, sp_count, tp_count),
+                        lax.axis_size(("sp", "tp")),
+                        axis=0,
+                    )
+                ),
+                ("sp", "tp"),
+                0,
+                0,
+            ),
+            axis=2,
         ),
         lax.all_to_all(
             to_pieces(rotary, sp_count, tp_count),

time: 55.9 us -> 74.4 us (1.33)
  local copies, waits for them, and re-layouts: 4.3 us -> 22.7 us
  waiting for transfers between devices: 2.64 us -> 1.38 us
  matrix products: 2.46 us -> 3.52 us
    unnamed x22 -> x51, local copies, waits for them, and re-layouts: 2.26 us -> 20.8 us
    dot_general x1, matrix products: 0.36 us -> 1.4 us  [shards(): jnp.einsum('shd,chd->shc', query_all, lookup_widening, preferred_element_...]
    all_to_all x1, waiting for transfers between devices: 2.41 us -> 1.38 us  [shards(): lax.all_to_all(jnp.stack(jnp.split(to_pieces(hidden_summary, sp_count, tp...]
  transfers between devices with their start and end apart: 2 -> 2, of which waited for: 2 -> 1; matrix products, arithmetic and copies ran while one was open for 7% -> 32% of each run, Pallas kernels for 0% -> 0%
where the time goes in v1:
time: 74.4 us; the launch traced here: 74.1 us
  blocking collectives  26.7 us (36%)
  local copies, waits for them, and re-layouts  22.7 us (31%)
  starting transfers between devices  13.2 us (18%)
  other arithmetic  4.95 us (7%)
  matrix products  3.52 us (5%)
  between operations  1.57 us (2%)
  waiting for transfers between devices  1.38 us (2%)
    unnamed x51, local copies, waits for them, and re-layouts  20.8 us
    psum x1, blocking collectives, shards(): lax.psum(partial_value.astype(jnp.bfloat16), 'tp').astype(jnp.float32)  10.6 us
    all_to_all x1, starting transfers between devices, shards(): lax.all_to_all(to_pieces(rotary, sp_count, tp_count), ('sp', 'tp'), split...  7.33 us
    all_to_all x1, starting transfers between devices, shards(): lax.all_to_all(jnp.stack(jnp.split(to_pieces(hidden_summary, sp_count, tp...  5.83 us
    unnamed x1, blocking collectives  5.76 us
    all_gather x1, blocking collectives, shards(): lax.all_gather(query_nope, 'tp', axis=1, tiled=True)  5.2 us
    all_gather x1, blocking collectives, shards(): lax.all_gather(query_rotary, 'tp', axis=1, tiled=True)  5.19 us
    reduce_sum x2, other arithmetic, rescaled_lines(): jnp.mean(vector * vector, axis=-1, keepdims=True) + norm_eps  1.81 us
  transfers between devices with their start and end apart: 2, of which 1 were waited for; matrix products, arithmetic and copies ran while one was open for 32% of the time, Pallas kernels for 0%

profile of v1, /device:TPU:0, one launch (start us, length us, event | category | flops | bytes accessed | tf_op | source)
XLA Modules:
  0.0 74.1 jit_solution(17798059621956757741)
XLA Ops:
  0.7 1.7 %fusion = f32[8,32]{1,0:T(8,128)S(1)} fusion(bf16[8,32,2048]{2,1,0:T(8,128)(2,1)} %param.9), kind=kLoop, calls=%fused_computation.2 | loop fusion | flops 1572608 | bytes 1049600 | tf_op jit(solution)/shard_map/reduce_sum | solution.py:18
  2.4 1.5 %fusion.2 = bf16[8,32,2048]{2,1,0:T(8,128)(2,1)S(1)} fusion(bf16[8,32,2048]{2,1,0:T(8,128)(2,1)} %param.9, f32[2048]{0:T(1024)} %param.10, f32[8,32]{1,0:T(8,128)S(1)} %add_rsqrt_fusion), kind=kLoop, calls=%fused_computation.4 | loop fusion | flops 2097152 | bytes 2106368 | tf_op jit(solution)/shard_map/convert_element_type | solution.py:62
  5.0 0.8 %reshape.296 = bf16[32,2,256]{2,1,0:T(2,128)(2,1)} reshape(bf16[32,1,16,32]{3,2,1,0:T(8,128)(2,1)S(1)} %bitcast.252) | data formatting | bytes 65536
  5.8 7.3 %all-to-all-start.1 = ((bf16[32,2,256]{2,1,0:T(2,128)(2,1)}), bf16[32,2,256]{2,1,0:T(2,128)(2,1)S(1)}, u32[]{:S(2)}, u32[]{:S(2)}) async-start(bf16[32,2,256]{2,1,0:T(2,128)(2,1)} %reshape.296), calls=%async_computation.1 | async-start | bytes 65536 | tf_op jit(solution)/shard_map/all_to_all | solution.py:97
  13.1 5.2 %all_gather.7 = bf16[1,16,64]{2,0,1:T(2,128)(2,1)S(1)} all-gather(bf16[1,4,64]{2,0,1:T(2,128)(2,1)S(1)} %copy.221), channel_id=1, replica_groups=mesh['sp'=8,'tp'=4] {'tp'}, dimensions={1}, use_global_device_ids=true | all-gather | bytes 2560 | tf_op jit(solution)/shard_map/all_gather | solution.py:112
  18.3 0.8 %multiply_reduce_fusion = (f32[256]{0:T(256)S(1)}, f32[256,512]{1,0:T(8,128)S(1)}) fusion(bf16[256,2048]{1,0:T(8,128)(2,1)S(1)} %bitcast.215, bf16[2048,512]{1,0:T(8,128)(2,1)S(1)} %copy-done), kind=kOutput, calls=%fused_computation.20 | convolution fusion | flops 537394944 | bytes 3671040 | tf_op jit(solution)/shard_map/dot_general | solution.py:64
  19.4 0.6 constant_dynamic-update-slice_fusion.31
  20.0 0.6 constant_dynamic-update-slice_fusion.30
  20.6 0.6 constant_dynamic-update-slice_fusion.29
  21.2 0.6 constant_dynamic-update-slice_fusion.28
  21.8 0.6 constant_dynamic-update-slice_fusion.27
  22.4 0.6 constant_dynamic-update-slice_fusion.26
  23.0 0.6 constant_dynamic-update-slice_fusion.25
  23.6 0.6 constant_dynamic-update-slice_fusion.24
  24.2 0.6 constant_dynamic-update-slice_fusion.23
  26.0 0.6 constant_dynamic-update-slice_fusion.20
  27.8 0.6 constant_dynamic-update-slice_fusion.17
  29.6 0.6 constant_dynamic-update-slice_fusion.14
  31.4 0.6 constant_dynamic-update-slice_fusion.11
  33.2 0.6 constant_dynamic-update-slice_fusion.8
  33.8 0.6 constant_dynamic-update-slice_fusion.7
  35.6 0.6 constant_dynamic-update-slice_fusion.4
  37.4 0.6 constant_dynamic-update-slice_fusion.1
  38.6 5.8 %all-to-all-start = ((bf16[32,1,1,32,128]{4,3,2,1,0:T(8,128)(2,1)}), bf16[32,1,1,32,128]{4,3,2,1,0:T(8,128)(2,1)S(1)}, u32[]{:S(2)}, u32[]{:S(2)}) async-start(bf16[32,1,1,32,128]{4,3,2,1,0:T(8,128)(2,1)} %constant_dynamic-update-slice_fusion), calls=%async_computation | async-start | bytes 524288 | tf_op jit(solution)/shard_map/all_to_all | solution.py:83
  45.8 5.2 %all_gather.6 = bf16[1,16,128]{2,0,1:T(2,128)(2,1)S(1)} all-gather(bf16[1,4,128]{2,0,1:T(2,128)(2,1)S(1)} %copy.220), channel_id=1, replica_groups=mesh['sp'=8,'tp'=4] {'tp'}, dimensions={1}, use_global_device_ids=true | all-gather | bytes 5120 | tf_op jit(solution)/shard_map/all_gather | solution.py:111
  51.1 1.4 %fusion.11 = f32[16,1,128]{2,1,0:T(1,128)S(1)} fusion(bf16[128,16,128]{2,1,0:T(8,128)(2,1)} %param.14, bf16[1,16,128]{2,0,1:T(2,128)(2,1)S(1)} %all_gather.6), kind=kOutput, calls=%fused_computation.17 | convolution fusion | flops 524288 | bytes 536576 | tf_op jit(solution)/shard_map/shd,chd->shc/dot_general | solution.py:114
  52.9 0.8 %squeeze.3 = bf16[1,1024,16]{1,2,0:T(8,128)(2,1)} reshape(bf16[32,1,32,16]{2,0,3,1:T(8,128)(2,1)S(1)} %copy.219) | data formatting | bytes 65536 | tf_op jit(solution)/shard_map/squeeze | solution.py:106
  53.6 1.4 %all-to-all-done = bf16[32,1,1,32,128]{4,3,2,1,0:T(8,128)(2,1)S(1)} async-done(((bf16[32,1,1,32,128]{4,3,2,1,0:T(8,128)(2,1)}), bf16[32,1,1,32,128]{4,3,2,1,0:T(8,128)(2,1)S(1)}, u32[]{:S(2)}, u32[]{:S(2)}) %all-to-all-start) | async-done | bytes 262176 | tf_op jit(solution)/shard_map/all_to_all | solution.py:83
  55.4 10.6 %psum.7 = bf16[1,16,1024]{2,1,0:T(8,128)(2,1)S(1)} all-reduce(bf16[1,16,1024]{2,1,0:T(8,128)(2,1)S(1)} %fusion.7), channel_id=1, replica_groups=mesh['sp'=8,'tp'=4] {'tp'}, use_global_device_ids=true, to_apply=%region_2.0 | all-reduce | flops 16384 | bytes 65536 | tf_op jit(solution)/shard_map/psum | solution.py:126
  66.8 5.8 %all-reduce = f32[16,1,128]{2,0,1:T(8,128)S(1)} all-reduce(f32[16,1,128]{2,0,1:T(8,128)S(1)} %bitcast.254), channel_id=2, replica_groups=mesh['sp'=8,'tp'=4] {'tp'}, use_global_device_ids=true, to_apply=%region_5.0.clone | all-reduce | flops 2048 | bytes 16384
  72.7 0.6 multiply_convert_fusion.1
  73.4 0.7 copy.271
  (61 shorter events, 12.7 us)
Async XLA Ops:
  0.6 17.7 %copy-start = (bf16[2048,512]{1,0:T(8,128)(2,1)S(1)}, bf16[2048,512]{1,0:T(8,128)(2,1)}, u32[]{:S(2)}) copy-start(bf16[2048,512]{1,0:T(8,128)(2,1)} %param.11) | copy-start | bytes 6291460
  0.6 3.3 %copy-start.1 = (bf16[2048,64]{0,1:T(8,128)(2,1)S(1)}, bf16[2048,64]{0,1:T(8,128)(2,1)}, u32[]{:S(2)}) copy-start(bf16[2048,64]{0,1:T(8,128)(2,1)} %param.12) | copy-start | bytes 786436
  2.4 10.7 %copy-start.3 = (bf16[1,4,64]{2,1,0:T(4,128)(2,1)S(1)}, bf16[1,4,64]{2,1,0:T(4,128)(2,1)}, u32[]{:S(2)}) copy-start(bf16[1,4,64]{2,1,0:T(4,128)(2,1)} %param.17) | copy-start | bytes 1540
  5.0 14.2 %copy-start.2 = (f32[512]{0:T(512)S(1)}, f32[512]{0:T(512)}, u32[]{:S(2)}) copy-start(f32[512]{0:T(512)} %param.13) | copy-start | bytes 6148
  5.8 32.9 %all-to-all-start.1 = ((bf16[32,2,256]{2,1,0:T(2,128)(2,1)}), bf16[32,2,256]{2,1,0:T(2,128)(2,1)S(1)}, u32[]{:S(2)}, u32[]{:S(2)}) async-start(bf16[32,2,256]{2,1,0:T(2,128)(2,1)} %reshape.296), calls=%async_computation.1 | async-start | bytes 65536 | tf_op jit(solution)/shard_map/all_to_all | solution.py:97
  19.1 25.4 %copy-start.4 = (bf16[1,4,128]{2,1,0:T(4,128)(2,1)S(1)}, bf16[1,4,128]{2,1,0:T(4,128)(2,1)}, u32[]{:S(2)}) copy-start(bf16[1,4,128]{2,1,0:T(4,128)(2,1)} %param.16) | copy-start | bytes 3076
  19.1 25.4 %copy-start.6 = (u32[32]{0:T(128)S(1)}, u32[32]{0:T(128)}, u32[]{:S(2)}) copy-start(u32[32]{0:T(128)} %constant.54) | copy-start | bytes 388
  19.4 47.2 %copy-start.5 = (bf16[128,16,128]{2,1,0:T(8,128)(2,1)S(1)}, bf16[128,16,128]{2,1,0:T(8,128)(2,1)}, u32[]{:S(2)}) copy-start(bf16[128,16,128]{2,1,0:T(8,128)(2,1)} %param.15) | copy-start | bytes 1572868
  38.6 16.4 %all-to-all-start = ((bf16[32,1,1,32,128]{4,3,2,1,0:T(8,128)(2,1)}), bf16[32,1,1,32,128]{4,3,2,1,0:T(8,128)(2,1)S(1)}, u32[]{:S(2)}, u32[]{:S(2)}) async-start(bf16[32,1,1,32,128]{4,3,2,1,0:T(8,128)(2,1)} %constant_dynamic-update-slice_fusion), calls=%async_computation | async-start | bytes 524288 | tf_op jit(solution)/shard_map/all_to_all | solution.py:83
